TPU v7x, 128 devices: a whole 4x4x4 slice. The times are simulated.
128 devices in a mesh: kv: 16 (over z, x), tp: 8 (over y, core).
Axes of the slice: x: 4, y: 4, z: 4, core: 2. Of those that a mesh axis runs over, the one named last changes fastest.
Arguments:
- hidden_in: bfloat16 [16, 4096], P(None, ('kv', 'tp')), may hold values from -5 to 5
- pre_gain: float32 [4096], P('kv'), may hold values from 0.1 to 1.9
- w_query: bfloat16 [4096, 3072], P('kv', 'tp'), may hold values from -0.09375 to 0.09375
- w_key: bfloat16 [4096, 1024], P('kv', 'tp'), may hold values from -0.09375 to 0.09375
- w_value: bfloat16 [4096, 1024], P('kv', 'tp'), may hold values from -0.09375 to 0.09375
- w_forget: bfloat16 [4096, 16], P('kv'), may hold values from -0.09375 to 0.09375
- forget_bias: float32 [16], P('tp'), may hold values from -2 to 1.5
- key_cache: bfloat16 [16, 16384, 1024], P(None, 'kv', 'tp'), may hold values from -1300 to 1300
- value_cache: bfloat16 [16, 16384, 1024], P(None, 'kv', 'tp'), may hold values from -6 to 6
- decay_to_end: float32 [16, 16, 16384], P(None, 'tp', 'kv'), may hold values from -16386 to 0, as said below
- w_output: bfloat16 [3072, 4096], P('tp', 'kv'), may hold values from -0.109375 to 0.109375
- mid_gain: float32 [4096], P('kv'), may hold values from 0.1 to 1.9
- w_gate: bfloat16 [4096, 11264], P('kv', 'tp'), may hold values from -0.09375 to 0.09375
- w_up: bfloat16 [4096, 11264], P('kv', 'tp'), may hold values from -0.09375 to 0.09375
- w_down: bfloat16 [11264, 4096], P('tp', 'kv'), may hold values from -0.0546875 to 0.0546875
Outputs:
- updated: float32 [16, 4096], P(None, ('kv', 'tp'))
Inputs may be any that keep to these rules, and one draw needn't show every extreme that they name: `decay_to_end`: never falls toward later positions and is 0 at the last cached position.
All inputs are finite; a program needn't handle non-finite values.
Results may differ from a plain program's by a relative error of at most 0.028.
Values may be sent and summed in bfloat16 or wider, within the bound.
A program may use at most 64 MiB of HBM per device.

v0:
```python
import jax
import jax.numpy as jnp
from jax import lax
from jax.sharding import Mesh
from jax.sharding import PartitionSpec as P

D = 4096
QH = 48
KEY_VALUE_HEADS = 16
HD = 64
KV = ("kv_0", "kv_1")
KV_TP = ("kv_0", "kv_1", "tp")


norm_eps = 1e-06


def in_order(parts, dim):
    parts = jnp.moveaxis(parts, 0, dim)
    dims = parts.shape
    return parts.reshape(*dims[:dim], dims[dim] * dims[dim + 1], *dims[dim + 2 :])


def sent_to_all(value, axis):
    peers = lax.axis_size(axis)
    return lax.all_to_all(
        jnp.broadcast_to(value[None], (peers, *value.shape)), axis, 0, 0, tiled=True
    )


def gather_directly(value, axis, dim):
    return in_order(sent_to_all(value, axis), dim)


def over_copies(value, axis):
    everything = sent_to_all(value, axis)
    return jnp.sum(everything, axis=0)


def in_one(arrays, axis):
    ravelled, at, finished = (jnp.concatenate([a.reshape(-1) for a in arrays]), 0, [])
    so_far = over_copies(ravelled, axis)
    for a in arrays:
        finished.append(so_far[at : at + a.size].reshape(a.shape))
        at += a.size
    return tuple(finished)


def collected_together(value, axis):
    leaves = jax.tree.leaves(value)
    sequence = sorted(range(len(leaves)), key=lambda k: -leaves[k].size)
    width = (1, *leaves[sequence[0]].shape)[-1]
    lines = [
        jnp.pad(leaves[k].reshape(-1), (0, -leaves[k].size % width)).reshape(-1, width)
        for k in sequence
    ]
    both, at, found = (lax.all_gather(jnp.concatenate(lines), axis), 0, {})
    for k, line in zip(sequence, lines):
        section = both[:, at : at + len(line)].reshape(len(both), -1)
        found[k] = section[:, : leaves[k].size].reshape(-1, *leaves[k].shape)
        at += len(line)
    numbers = iter(range(len(leaves)))
    return jax.tree.map(lambda _: found[next(numbers)], value)


def joined_all(value, axes, combine):
    for axis in axes:
        pieces = collected_together(value, axis)
        value = jax.tree.map(lambda part: part[0], pieces)
        for k in range(1, lax.axis_size(axis)):
            value = combine(value, jax.tree.map(lambda part: part[k], pieces))
    return value


def over_copies_2(value, axis):
    return sent_to_all(value, axis).astype(jnp.float32).sum(axis=0)


def cut_along(value, dim, peers):
    dims = value.shape
    parts = value.reshape(*dims[:dim], peers, dims[dim] // peers, *dims[dim + 1 :])
    return jnp.moveaxis(parts, dim, 0)


def sum_at_owner(value, axis, dim):
    parts = cut_along(value, dim, lax.axis_size(axis))
    arrived = lax.all_to_all(parts, axis, split_axis=0, concat_axis=0, tiled=True)
    return arrived.astype(jnp.float32).sum(axis=0)


def combine_parts(first, second):
    max_first, sum_first, acc_first = first
    max_second, sum_second, acc_second = second
    larger = jnp.maximum(max_first, max_second)
    scale_first = jnp.exp(max_first - larger)
    scale_second = jnp.exp(max_second - larger)
    return (
        larger,
        sum_first * scale_first + sum_second * scale_second,
        acc_first * scale_first[..., None] + acc_second * scale_second[..., None],
    )


def project_block(scaled, w_query, w_key, w_value, w_forget):
    q_part = jnp.dot(scaled, w_query, preferred_element_type=jnp.float32)
    k_part = jnp.dot(scaled, w_key, preferred_element_type=jnp.float32)
    v_part = jnp.dot(scaled, w_value, preferred_element_type=jnp.float32)
    f_part = jnp.dot(scaled, w_forget, preferred_element_type=jnp.float32)
    return (q_part, k_part, v_part, f_part)


def on_device(
    hidden_in,
    pre_gain,
    w_query,
    w_key,
    w_value,
    w_forget,
    forget_bias,
    key_cache,
    value_cache,
    decay_to_end,
    w_output,
    mid_gain,
    w_gate,
    w_up,
    w_down,
):
    batch_rows = hidden_in.shape[0]
    kv_here = decay_to_end.shape[1]
    positions = decay_to_end.shape[2]
    group_size = QH // KEY_VALUE_HEADS
    tp_pos = lax.axis_index("tp")
    col_block = gather_directly(hidden_in, "tp", 1).astype(jnp.float32)
    scaled = (col_block * pre_gain).astype(jnp.bfloat16)
    square = jnp.sum(col_block * col_block, axis=1, keepdims=True)
    q_part, k_part, v_part, f_part = project_block(scaled, w_query, w_key, w_value, w_forget)
    q_sum, k_sum, v_sum, f_sum, square_all = in_one((q_part, k_part, v_part, f_part, square), KV)
    inv_rms = lax.rsqrt(square_all / D + norm_eps)
    query = (q_sum * inv_rms).astype(jnp.bfloat16).reshape(batch_rows, kv_here, group_size, HD)
    key_new = (k_sum * inv_rms).astype(jnp.bfloat16).reshape(batch_rows, kv_here, HD)
    value_new = (v_sum * inv_rms).astype(jnp.bfloat16).reshape(batch_rows, kv_here, HD)
    forget_mine = lax.dynamic_slice_in_dim(f_sum * inv_rms, tp_pos * kv_here, kv_here, 1)
    log_new = jax.nn.log_sigmoid(forget_mine + forget_bias)
    score_scale = HD ** (-0.5)
    key_rows = key_cache.reshape(batch_rows, positions, kv_here, HD)
    value_rows = value_cache.reshape(batch_rows, positions, kv_here, HD)
    scores = (
        jnp.einsum("bgqd,bpgd->bgqp", query, key_rows, preferred_element_type=jnp.float32)
        * score_scale
    )
    scores = scores + log_new[:, :, None, None] + decay_to_end[:, :, None, :]
    local_max = jnp.max(scores, axis=3)
    weights = jnp.exp(scores - local_max[..., None])
    local_sum = jnp.sum(weights, axis=3)
    local_acc = jnp.einsum(
        "bgqp,bpgd->bgqd",
        weights.astype(jnp.bfloat16),
        value_rows,
        preferred_element_type=jnp.float32,
    )
    run_max, run_sum, run_acc = joined_all((local_max, local_sum, local_acc), KV, combine_parts)
    own_score = (
        jnp.einsum("bgqd,bgd->bgq", query, key_new, preferred_element_type=jnp.float32)
        * score_scale
    )
    larger = jnp.maximum(run_max, own_score)
    keep_factor = jnp.exp(run_max - larger)
    own_weight = jnp.exp(own_score - larger)
    total = run_sum * keep_factor + own_weight
    attended = (
        run_acc * keep_factor[..., None]
        + own_weight[..., None] * value_new.astype(jnp.float32)[:, :, None, :]
    ) / total[..., None]
    attended = attended.astype(jnp.bfloat16).reshape(batch_rows, kv_here * group_size * HD)
    out_part = jnp.dot(attended, w_output, preferred_element_type=jnp.float32)
    out_block = over_copies_2(out_part.astype(jnp.bfloat16), "tp").astype(jnp.float32)
    mid_block = col_block + out_block
    own_width = hidden_in.shape[1]
    residual_mine = lax.dynamic_slice_in_dim(mid_block, tp_pos * own_width, own_width, 1)
    mid_scaled = (mid_block * mid_gain).astype(jnp.bfloat16)
    mid_square = jnp.sum(mid_block * mid_block, axis=1, keepdims=True)
    gate_part = jnp.dot(mid_scaled, w_gate, preferred_element_type=jnp.float32)
    up_part = jnp.dot(mid_scaled, w_up, preferred_element_type=jnp.float32)
    gate_sum, up_sum, mid_total = in_one((gate_part, up_part, mid_square), KV)
    mid_inv = lax.rsqrt(mid_total / D + norm_eps)
    hidden_units = (jax.nn.silu(gate_sum * mid_inv) * (up_sum * mid_inv)).astype(jnp.bfloat16)
    down_part = jnp.dot(hidden_units, w_down, preferred_element_type=jnp.float32)
    down_sum = sum_at_owner(down_part.astype(jnp.bfloat16), "tp", 1)
    return residual_mine + down_sum


def solution(mesh):
    split = Mesh(mesh.devices.reshape(4, 4, mesh.shape["tp"]), ("kv_0", "kv_1", "tp"))
    return jax.shard_map(
        on_device,
        mesh=split,
        in_specs=(
            P(None, KV_TP),
            P(KV),
            P(KV, "tp"),
            P(KV, "tp"),
            P(KV, "tp"),
            P(KV, None),
            P("tp"),
            P(None, KV, "tp"),
            P(None, KV, "tp"),
            P(None, "tp", KV),
            P("tp", KV),
            P(KV),
            P(KV, "tp"),
            P(KV, "tp"),
            P("tp", KV),
        ),
        out_specs=P(None, KV_TP),
        check_vma=False,
    )
```

profile of v0, /device:TPU:1, one launch (start us, length us, event | category | flops | bytes accessed | tf_op | source)
XLA Modules:
  0.0 144.4 jit_solution(15957506120397511670)
XLA Ops:
  0.0 0.8 broadcast_in_dim.8
  0.9 10.4 %all_to_all.27 = bf16[8,2,256]{2,1,0:T(2,128)(2,1)S(1)} all-to-all(bf16[8,2,256]{2,1,0:T(2,128)(2,1)S(1)} %reshape.501), channel_id=1, replica_groups=mesh['kv_0'=4,'kv_1'=4,'tp'=8] {'tp'}, dimensions={0} | all-to-all | bytes 16384 | tf_op jit(solution)/shard_map/all_to_all | solution.py:26
  11.6 0.7 multiply_convert_fusion.6
  12.3 0.8 fusion.58
  13.2 1.1 fusion.57
  14.3 1.0 fusion.3
  15.3 1.0 fusion.2
  16.3 1.3 broadcast_in_dim.9
  17.5 7.6 %all-to-all-start.1 = ((f32[16,1,10512]{2,1,0:T(1,128)}), f32[16,1,10512]{2,1,0:T(1,128)S(1)}, u32[]{:S(2)}, u32[]{:S(2)}) async-start(f32[16,1,10512]{2,1,0:T(1,128)} %broadcast_in_dim.9), calls=%async_computation.1 | async-start | bytes 1359872 | tf_op jit(solution)/shard_map/all_to_all | solution.py:26
  25.1 6.4 %copy.62 = bf16[16,1024,128]{1,2,0:T(8,128)(2,1)} copy(bf16[16,1024,128]{2,1,0:T(8,128)(2,1)} %param.22) | data formatting | bytes 8388608 | tf_op args[7]
  31.5 6.5 %copy.63 = bf16[16,1024,128]{1,2,0:T(8,128)(2,1)} copy(bf16[16,1024,128]{2,1,0:T(8,128)(2,1)} %param.23) | data formatting | bytes 8388608 | tf_op args[8]
  38.0 0.4 reduce_sum.66
  38.9 2.9 %fusion.56 = (f32[16,2,3]{2,1,0:T(2,128)S(1)}, f32[16,2,3,1024]{3,2,1,0:T(4,128)S(1)}) fusion(f32[16,2,1024]{2,1,0:T(2,128)S(1)} %copy-done.4, f32[16,2]{1,0:T(8,128)S(1)} %fusion.24, bf16[16,2,3,64]{3,2,1,0:T(4,128)(2,1)S(1)} %multiply_convert_fusion.1, bf16[16,1024,2,64]{1,3,2,0:T(8,128)(2,1)} %bitcast.135), kind=kOutput, calls=%fused_computation.115 | convolution fusion | flops 12976032 | bytes 4731392 | tf_op jit(solution)/shard_map/bgqd,bpgd->bgqp/dot_general | solution.py:149
  42.6 3.5 %fusion.6 = f32[16,2,3,64]{3,2,1,0:T(4,128)S(1)} fusion(bf16[16,1024,2,64]{1,3,2,0:T(8,128)(2,1)} %bitcast.136, f32[16,2,3,1024]{3,2,1,0:T(4,128)S(1)} %get-tuple-element.45, f32[16,2,3]{2,1,0:T(2,128)S(1)} %get-tuple-element.44), kind=kOutput, calls=%fused_computation.12 | convolution fusion | flops 12779520 | bytes 4612480 | tf_op jit(solution)/shard_map/bgqp,bpgd->bgqd/dot_general | solution.py:156
  46.2 10.0 %all-gather.2 = f32[4,100,64]{1,2,0:T(8,128)S(1)} all-gather(f32[1,100,64]{1,2,0:T(8,128)S(1)} %copy.64), channel_id=2, replica_groups=mesh['kv_0'=4,'kv_1'=4,'tp'=8] {'kv_0'}, dimensions={0}, use_global_device_ids=true | all-gather | bytes 128000 | tf_op jit(solution)/shard_map/all_gather | solution.py:57
  57.2 9.4 %all-gather.3 = f32[4,100,64]{1,2,0:T(8,128)S(1)} all-gather(f32[1,100,64]{1,2,0:T(8,128)S(1)} %maximum_bitcast_fusion.1), channel_id=3, replica_groups=mesh['kv_0'=4,'kv_1'=4,'tp'=8] {'kv_1'}, dimensions={0}, use_global_device_ids=true | all-gather | bytes 128000 | tf_op jit(solution)/shard_map/all_gather | solution.py:57
  71.3 13.9 %all_to_all.28 = bf16[8,16,256]{2,1,0:T(8,128)(2,1)S(1)} all-to-all(bf16[8,16,256]{2,1,0:T(8,128)(2,1)S(1)} %broadcast_in_dim.10), channel_id=1, replica_groups=mesh['kv_0'=4,'kv_1'=4,'tp'=8] {'tp'}, dimensions={0} | all-to-all | bytes 131072 | tf_op jit(solution)/shard_map/all_to_all | solution.py:26
  86.1 1.5 %broadcast_in_dim.11 = f32[16,1,45072]{2,1,0:T(1,128)S(1)} broadcast(f32[45072]{0:T(1024)S(1)} %pad_maximum_fusion), dimensions={2} | broadcast | bytes 3064896 | tf_op jit(solution)/shard_map/broadcast_in_dim | solution.py:27
  87.6 41.5 %all_to_all.29 = f32[16,1,45072]{2,1,0:T(1,128)} all-to-all(f32[16,1,45072]{2,1,0:T(1,128)S(1)} %broadcast_in_dim.11), channel_id=1, replica_groups=mesh['kv_0'=4,'kv_1'=4,'tp'=8] {'kv_0','kv_1'}, dimensions={0} | all-to-all | bytes 5769216 | tf_op jit(solution)/shard_map/all_to_all | solution.py:26
  129.1 3.6 %reduce_sum.71 = f32[45072]{0:T(1024)S(1)} reduce(f32[16,1,45072]{2,1,0:T(1,128)} %all_to_all.29, f32[]{:T(128)} %constant.12.clone.1), dimensions={0,1}, to_apply=%region_6.7 | reduce | flops 676080 | bytes 3064900 | tf_op jit(solution)/shard_map/reduce_sum | solution.py:37
  133.2 0.7 reshape.503
  133.9 5.1 %all-to-all-start.4 = ((bf16[8,2,256]{2,1,0:T(2,128)(2,1)}), bf16[8,2,256]{2,1,0:T(2,128)(2,1)S(1)}, u32[]{:S(2)}, u32[]{:S(2)}) async-start(bf16[8,2,256]{2,1,0:T(2,128)(2,1)} %reshape.503), calls=%async_computation.4 | async-start | bytes 16384 | tf_op jit(solution)/shard_map/all_to_all | solution.py:87
  139.0 4.6 %all-to-all-done.4 = bf16[8,2,256]{2,1,0:T(2,128)(2,1)S(1)} async-done(((bf16[8,2,256]{2,1,0:T(2,128)(2,1)}), bf16[8,2,256]{2,1,0:T(2,128)(2,1)S(1)}, u32[]{:S(2)}, u32[]{:S(2)}) %all-to-all-start.4) | async-done | bytes 8224 | tf_op jit(solution)/shard_map/all_to_all | solution.py:87
  143.7 0.7 dynamic-slice_add_fusion
  (123 shorter events, 8.6 us)
Async XLA Ops:
  0.0 85.6 %copy-start = (bf16[256,1408]{1,0:T(8,128)(2,1)S(1)}, bf16[256,1408]{1,0:T(8,128)(2,1)}, u32[]{:S(2)}) copy-start(bf16[256,1408]{1,0:T(8,128)(2,1)} %param.28) | copy-start | bytes 2162692
  17.5 20.5 %all-to-all-start.1 = ((f32[16,1,10512]{2,1,0:T(1,128)}), f32[16,1,10512]{2,1,0:T(1,128)S(1)}, u32[]{:S(2)}, u32[]{:S(2)}) async-start(f32[16,1,10512]{2,1,0:T(1,128)} %broadcast_in_dim.9), calls=%async_computation.1 | async-start | bytes 1359872 | tf_op jit(solution)/shard_map/all_to_all | solution.py:26
  31.5 7.2 %copy-start.6 = (f32[2]{0:T(128)S(1)}, f32[2]{0:T(128)}, u32[]{:S(2)}) copy-start(f32[2]{0:T(128)} %param.21) | copy-start | bytes 28
  31.5 7.3 %copy-start.4 = (f32[16,2,1024]{2,1,0:T(2,128)S(1)}, f32[16,2,1024]{2,1,0:T(2,128)}, u32[]{:S(2)}) copy-start(f32[16,2,1024]{2,1,0:T(2,128)} %param.24) | copy-start | bytes 393220
  42.6 28.6 %copy-start.3 = (bf16[384,256]{1,0:T(8,128)(2,1)S(1)}, bf16[384,256]{1,0:T(8,128)(2,1)}, u32[]{:S(2)}) copy-start(bf16[384,256]{1,0:T(8,128)(2,1)} %param.25) | copy-start | bytes 589828
  46.1 39.5 %copy-start.5 = (f32[256]{0:T(256)S(1)}, f32[256]{0:T(256)}, u32[]{:S(2)}) copy-start(f32[256]{0:T(256)} %param.26) | copy-start | bytes 3076
  46.1 39.8 %copy-start.1 = (bf16[256,1408]{1,0:T(8,128)(2,1)S(1)}, bf16[256,1408]{1,0:T(8,128)(2,1)}, u32[]{:S(2)}) copy-start(bf16[256,1408]{1,0:T(8,128)(2,1)} %param.27) | copy-start | bytes 2162692
  87.6 45.2 %copy-start.2 = (bf16[1408,256]{1,0:T(8,128)(2,1)S(1)}, bf16[1408,256]{1,0:T(8,128)(2,1)}, u32[]{:S(2)}) copy-start(bf16[1408,256]{1,0:T(8,128)(2,1)} %param.29) | copy-start | bytes 2162692
  133.9 9.7 %all-to-all-start.4 = ((bf16[8,2,256]{2,1,0:T(2,128)(2,1)}), bf16[8,2,256]{2,1,0:T(2,128)(2,1)S(1)}, u32[]{:S(2)}, u32[]{:S(2)}) async-start(bf16[8,2,256]{2,1,0:T(2,128)(2,1)} %reshape.503), calls=%async_computation.4 | async-start | bytes 16384 | tf_op jit(solution)/shard_map/all_to_all | solution.py:87
where the time goes:
time: 145 us; the launch traced here: 144 us
  blocking collectives  85.3 us (59%)
  local copies, waits for them, and re-layouts  23.3 us (16%)
  starting transfers between devices  12.7 us (9%)
  matrix products  11.2 us (8%)
  other arithmetic  6.83 us (5%)
  waiting for transfers between devices  4.64 us (3%)
    all_to_all x3, blocking collectives, sent_to_all(): lax.all_to_all(jnp.broadcast_to(value[None], (peers, *value.shape)), axis...  65.8 us
    all_gather x2, blocking collectives, collected_together(): both, at, found = (lax.all_gather(jnp.concatenate(lines), axis), 0, {})  19.4 us
    unnamed x23, local copies, waits for them, and re-layouts  14 us
    all_to_all x1, starting transfers between devices, sent_to_all(): lax.all_to_all(jnp.broadcast_to(value[None], (peers, *value.shape)), axis...  7.6 us
    all_to_all x1, starting transfers between devices, sum_at_owner(): lax.all_to_all(parts, axis, split_axis=0, concat_axis=0, tiled=True)  5.06 us
    all_to_all x1, waiting for transfers between devices, sum_at_owner(): lax.all_to_all(parts, axis, split_axis=0, concat_axis=0, tiled=True)  4.64 us
    reduce_sum x2, other arithmetic, over_copies(): return jnp.sum(everything, axis=0)  4.04 us
    broadcast_in_dim x4, local copies, waits for them, and re-layouts, sent_to_all(): jnp.broadcast_to(value[None], (peers, *value.shape))  3.51 us
  transfers between devices with their start and end apart: 2, of which 1 were waited for; matrix products, arithmetic and copies ran while one was open for 9% of the time, Pallas kernels for 0%

commit v1 on v0

v1 whole, which is shorter than its diff:
```python
import functools

import jax
import jax.numpy as jnp
from jax import lax
from jax.experimental import pallas as pl
from jax.experimental.pallas import tpu as pltpu
from jax.sharding import PartitionSpec as P

D = 4096
QH = 48
KEY_VALUE_HEADS = 16
HD = 64
NORM_EPS = 1e-06
MESH = pl.DeviceIdType.MESH
F32 = jnp.float32
BF16 = jnp.bfloat16


def kernel(
    n_kv,
    n_tp,
    hidden_in,
    pre_gain,
    w_query,
    w_key,
    w_value,
    w_forget,
    forget_bias,
    key_cache,
    value_cache,
    decay,
    w_output,
    mid_gain,
    w_gate,
    w_up,
    w_down,
    out_ref,
    xs,
    pg,
    wq,
    wk,
    wv,
    wf,
    fb,
    kc,
    vc,
    dec,
    wo,
    mg,
    wg,
    wu,
    wd,
    load_sem,
    dec_rows,
    q_mine,
    q_in,
    s_mine,
    s_in,
    t_mine,
    t_in,
    q_rows,
    o_rows,
    l_rows,
    a_mine,
    a_in,
    e_mine,
    e_in,
    p_mine,
    p_in,
    g_rows,
    g_mine,
    g_in,
    h_all,
    h_rows,
    d_mine,
    d_in,
    x_send,
    x_recv,
    q_send,
    q_recv,
    s_send,
    s_recv,
    t_send,
    t_recv,
    a_send,
    a_recv,
    e_send,
    e_recv,
    p_send,
    p_recv,
    g_send,
    g_recv,
    h_send,
    h_recv,
    d_send,
    d_recv,
):
    kv = lax.axis_index("kv")
    tp = lax.axis_index("tp")
    kv_peers = [lax.rem(kv + d, n_kv) for d in range(1, n_kv)]
    tp_peers = [lax.rem(tp + d, n_tp) for d in range(1, n_tp)]

    loads = [
        (hidden_in, xs.at[tp]),
        (pre_gain, pg),
        (w_query, wq),
        (w_key, wk),
        (w_value, wv),
        (w_forget, wf),
        (forget_bias, fb),
        (decay, dec),
        (key_cache, kc),
        (value_cache, vc),
        (w_output, wo),
        (mid_gain, mg),
        (w_gate, wg),
        (w_up, wu),
        (w_down, wd),
    ]
    loads = [pltpu.make_async_copy(a, b, load_sem.at[i]) for i, (a, b) in enumerate(loads)]
    for copy in loads:
        copy.start()
    (l_x, l_pg, l_wq, l_wk, l_wv, l_wf, l_fb, l_dec, l_kc, l_vc, l_wo, l_mg, l_wg, l_wu, l_wd) = loads

    barrier = pltpu.get_barrier_semaphore()
    for peer in kv_peers:
        pl.semaphore_signal(barrier, inc=1, device_id={"kv": peer, "tp": tp}, device_id_type=MESH)
    for peer in tp_peers:
        pl.semaphore_signal(barrier, inc=1, device_id={"kv": kv, "tp": peer}, device_id_type=MESH)
    pl.semaphore_wait(barrier, n_kv + n_tp - 2)

    def send(axis, src, dst, send_sem, recv_sem):
        peers = kv_peers if axis == "kv" else tp_peers
        copies = []
        for i, peer in enumerate(peers):
            device = {"kv": peer, "tp": tp} if axis == "kv" else {"kv": kv, "tp": peer}
            copy = pltpu.make_async_remote_copy(
                src_ref=src(peer),
                dst_ref=dst(i),
                send_sem=send_sem.at[i],
                recv_sem=recv_sem.at[i],
                device_id=device,
                device_id_type=MESH,
            )
            copy.start()
            copies.append(copy)
        return copies

    def received(copies):
        for copy in copies:
            copy.wait_recv()

    def sent(copies):
        for copy in copies:
            copy.wait_send()

    lane = lax.broadcasted_iota(jnp.int32, (16, 128), 1)
    low = lane < 64

    l_x.wait()
    x_copies = send("tp", lambda peer: xs.at[tp], lambda i: xs.at[tp], x_send, x_recv)

    q_rows[...] = jnp.zeros_like(q_rows)
    l_dec.wait()
    row = lax.broadcasted_iota(jnp.int32, (8, 1024), 0)
    for b in range(16):
        dec_rows[b] = jnp.where(row < 3, dec[b, 0:1, :], dec[b, 1:2, :])
    for copy in (l_pg, l_wq, l_wk, l_wv, l_wf, l_fb):
        copy.wait()

    received(x_copies)
    x = jnp.concatenate([xs[t].astype(F32) for t in range(n_tp)], axis=1)
    scaled = (x * pg[...]).astype(BF16)
    q_part = jnp.dot(scaled, wq[...], preferred_element_type=F32)
    q_mine[...] = q_part
    square = jnp.sum(x * x, axis=1, keepdims=True)
    square = jnp.broadcast_to(square, (16, 128))
    s_mine[...] = jnp.where(low[0:8], square[0:8], square[8:16])
    q_copies = send("kv", lambda peer: q_mine, lambda i: q_in.at[i], q_send, q_recv)
    s_copies = send("kv", lambda peer: s_mine, lambda i: s_in.at[i], s_send, s_recv)

    k_part = jnp.dot(scaled, wk[...], preferred_element_type=F32)
    v_part = jnp.dot(scaled, wv[...], preferred_element_type=F32)
    f_part = jnp.dot(scaled, wf[...], preferred_element_type=F32)
    f_col = lax.broadcasted_iota(jnp.int32, (16, 16), 1)
    f_zero = jnp.zeros_like(f_part)
    f_first = jnp.sum(jnp.where(f_col == 2 * tp, f_part, f_zero), axis=1, keepdims=True)
    f_second = jnp.sum(jnp.where(f_col == 2 * tp + 1, f_part, f_zero), axis=1, keepdims=True)
    f_wide = jnp.where(low, f_first, f_second)
    t_mine[pl.ds(0, 16, stride=8), :] = k_part
    t_mine[pl.ds(1, 16, stride=8), :] = v_part
    t_mine[pl.ds(2, 16, stride=8), :] = f_wide
    t_mine[pl.ds(3, 16, stride=8), :] = square
    t_copies = send(
        "kv", lambda peer: t_mine.at[pl.ds(pl.multiple_of(peer * 8, 8), 8)], lambda i: t_in.at[i], t_send, t_recv
    )
    sent(x_copies)
    l_kc.wait()
    l_vc.wait()

    received(q_copies)
    received(s_copies)
    q_sum = q_mine[...]
    s_sum = s_mine[...]
    for i in range(n_kv - 1):
        q_sum = q_sum + q_in[i]
        s_sum = s_sum + s_in[i]
    s_sum = jnp.concatenate([s_sum[:, 0:1], s_sum[:, 64:65]], axis=0)
    inv_rms = lax.rsqrt(s_sum / D + NORM_EPS)
    query = (q_sum * inv_rms).astype(BF16).astype(F32) * (HD**-0.5)
    zero = jnp.zeros((16, 128), F32)
    for h in range(6):
        c, half, g = h // 2, h % 2, h // 3
        part = query[:, c * 128 : (c + 1) * 128]
        if half != g:
            part = pltpu.roll(part, 64, 1)
        q_rows[pl.ds(h, 16, stride=8), :] = jnp.where(low if g == 0 else ~low, part, zero)

    received(t_copies)
    t_sum = t_mine[pl.ds(pl.multiple_of(kv * 8, 8), 8), :]
    for i in range(n_kv - 1):
        t_sum = t_sum + t_in[i]
    t_inv = lax.rsqrt(t_sum[3:4, :] / D + NORM_EPS)
    key_new = (t_sum[0:1, :] * t_inv).astype(BF16).astype(F32)
    value_new = (t_sum[1:2, :] * t_inv).astype(BF16).astype(F32)
    low8 = low[0:8]
    row8 = lax.broadcasted_iota(jnp.int32, (8, 128), 0)
    gate_in = t_sum[2:3, :] * t_inv + jnp.where(low[0:1], fb[0:1, 0:1], fb[0:1, 1:2])
    log_new = jnp.minimum(gate_in, 0.0) - jnp.log1p(jnp.exp(-jnp.abs(gate_in)))
    q_own = q_rows[pl.ds(pl.multiple_of(kv * 8, 8), 8), :]
    own = jnp.sum(q_own * key_new, axis=1, keepdims=True)
    own = own - jnp.where(row8[:, 0:1] < 3, log_new[:, 0:1], log_new[:, 64:65])

    for b in range(16):
        q8 = q_rows[b * 8 : (b + 1) * 8, :].astype(BF16)
        scores = lax.dot_general(q8, kc[b], (((1,), (1,)), ((), ())), preferred_element_type=F32)
        scores = scores + dec_rows[b]
        own_b = jnp.where(kv == b, own, -jnp.inf)
        top = jnp.maximum(jnp.max(scores, axis=1, keepdims=True), own_b)
        weights = jnp.exp(scores - top)
        own_weight = jnp.exp(own_b - top)
        total = jnp.sum(weights, axis=1, keepdims=True) + own_weight
        mixed = jnp.dot(weights.astype(BF16), vc[b], preferred_element_type=F32)
        mixed = mixed + own_weight * value_new
        o_rows[b * 8 : (b + 1) * 8, :] = mixed / total
        l_rows[b * 8 : (b + 1) * 8, :] = jnp.broadcast_to(top + jnp.log(total), (8, 128))

    heads = [o_rows[pl.ds(h, 16, stride=8), :] for h in range(6)]
    logs = [l_rows[pl.ds(h, 16, stride=8), :] for h in range(6)]
    chunk_0 = jnp.where(low, heads[0], pltpu.roll(heads[1], 64, 1))
    chunk_1 = jnp.where(low, heads[2], heads[3])
    chunk_2 = jnp.where(low, pltpu.roll(heads[4], 64, 1), heads[5])
    mine = jnp.concatenate([chunk_0, chunk_1, chunk_2], axis=1).astype(BF16)
    a_mine[...] = mine
    e_wide = logs[0]
    for h in range(1, 6):
        e_wide = jnp.where(lane < 16 * h, e_wide, logs[h])
    e_mine[...] = e_wide
    e_copies = send("kv", lambda peer: e_mine, lambda i: e_in.at[i], e_send, e_recv)
    a_copies = send("kv", lambda peer: a_mine, lambda i: a_in.at[i], a_send, a_recv)
    sent(q_copies)
    sent(s_copies)
    sent(t_copies)
    received(e_copies)
    parts = [e_wide] + [e_in[i] for i in range(n_kv - 1)]
    top = functools.reduce(jnp.maximum, parts)
    shares = [jnp.exp(part - top) for part in parts]
    whole = functools.reduce(jnp.add, shares)
    inverse = 1.0 / whole
    l_wo.wait()
    received(a_copies)
    attended = jnp.zeros((16, 384), F32)
    for i in range(n_kv):
        share = shares[i] * inverse
        wide = jnp.concatenate(
            [jnp.broadcast_to(share[:, 16 * h : 16 * h + 1], (16, 128)) for h in range(6)], axis=1
        )
        wide = jnp.concatenate(
            [
                jnp.where(low, wide[:, 256 * c : 256 * c + 128], wide[:, 256 * c + 128 : 256 * c + 256])
                for c in range(3)
            ],
            axis=1,
        )
        value = mine if i == 0 else a_in[i - 1]
        attended = attended + wide * value.astype(F32)

    part = jnp.dot(attended.astype(BF16), wo[...], preferred_element_type=F32).astype(BF16)
    p_mine[...] = part
    p_copies = send("tp", lambda peer: p_mine, lambda i: p_in.at[i], p_send, p_recv)
    sent(e_copies)
    sent(a_copies)
    for copy in (l_mg, l_wg, l_wu, l_wd):
        copy.wait()
    received(p_copies)
    projected = part.astype(F32)
    for i in range(n_tp - 1):
        projected = projected + p_in[i].astype(F32)
    mid = x + projected
    mid_scaled = (mid * mg[...]).astype(BF16)
    gate_part = jnp.dot(mid_scaled, wg[...], preferred_element_type=F32)
    up_part = jnp.dot(mid_scaled, wu[...], preferred_element_type=F32)
    mid_square = jnp.broadcast_to(jnp.sum(mid * mid, axis=1, keepdims=True), (16, 128))
    square_high = mid_square.astype(BF16).astype(F32)
    for c in range(11):
        g_rows[pl.ds(c, 16, stride=24), :] = gate_part[:, 128 * c : 128 * (c + 1)]
        g_rows[pl.ds(11 + c, 16, stride=24), :] = up_part[:, 128 * c : 128 * (c + 1)]
    g_rows[pl.ds(22, 16, stride=24), :] = square_high
    g_rows[pl.ds(23, 16, stride=24), :] = mid_square - square_high
    for b in range(16):
        g_mine[b] = g_rows[24 * b : 24 * (b + 1), :].astype(BF16)
    g_copies = send("kv", lambda peer: g_mine.at[peer], lambda i: g_in.at[i], g_send, g_recv)
    sent(p_copies)
    received(g_copies)
    g_sum = g_mine[kv].astype(F32)
    for i in range(n_kv - 1):
        g_sum = g_sum + g_in[i].astype(F32)
    mid_inv = lax.rsqrt((g_sum[22:23, :] + g_sum[23:24, :]) / D + NORM_EPS)
    gate = g_sum[0:11, :] * mid_inv
    up = g_sum[11:22, :] * mid_inv
    hidden = gate / (1.0 + jnp.exp(-gate)) * up
    hidden = jnp.concatenate([hidden, jnp.zeros((5, 128), F32)], axis=0).astype(BF16)
    h_all[kv] = hidden
    h_copies = send("kv", lambda peer: h_all.at[kv], lambda i: h_all.at[kv], h_send, h_recv)
    sent(g_copies)
    received(h_copies)
    for b in range(16):
        h_rows[16 * b : 16 * (b + 1), :] = h_all[b].astype(F32)
    units = jnp.concatenate([h_rows[pl.ds(c, 16, stride=16), :] for c in range(11)], axis=1).astype(BF16)
    down = jnp.dot(units, wd[...], preferred_element_type=F32).astype(BF16)
    d_mine[0] = down[:, 0:128]
    d_mine[1] = down[:, 128:256]
    d_copies = send("tp", lambda peer: d_mine.at[peer // 4], lambda i: d_in.at[i], d_send, d_recv)
    sent(h_copies)
    result = d_mine[tp // 4].astype(F32)
    received(d_copies)
    for i in range(n_tp - 1):
        result = result + d_in[i].astype(F32)
    result = jnp.where(tp < 4, mid[:, 0:128], mid[:, 128:256]) + result
    place = lax.rem(tp, 4)
    pick = result[:, 0:32]
    for r in range(1, 4):
        pick = jnp.where(place == r, result[:, 32 * r : 32 * (r + 1)], pick)
    out_ref[...] = pick
    sent(d_copies)


def on_device(n_kv, n_tp, *args):
    args = list(args)
    for i in (1, 6, 11):
        args[i] = args[i].reshape(1, -1)
    vmem = pltpu.VMEM
    own = [vmem(a.shape, a.dtype) for a in args[1:]]
    kv_other, tp_other = n_kv - 1, n_tp - 1
    dma = pltpu.SemaphoreType.DMA
    scratch = [
        vmem((n_tp, 16, 32), BF16),
        *own,
        dma((15,)),
        vmem((16, 8, 1024), F32),
        vmem((16, 384), F32),
        vmem((kv_other, 16, 384), F32),
        vmem((8, 128), F32),
        vmem((kv_other, 8, 128), F32),
        vmem((128, 128), F32),
        vmem((kv_other, 8, 128), F32),
        vmem((128, 128), F32),
        vmem((128, 128), F32),
        vmem((128, 128), F32),
        vmem((16, 384), BF16),
        vmem((kv_other, 16, 384), BF16),
        vmem((16, 128), F32),
        vmem((kv_other, 16, 128), F32),
        vmem((16, 256), BF16),
        vmem((tp_other, 16, 256), BF16),
        vmem((16 * 24, 128), F32),
        vmem((16, 24, 128), BF16),
        vmem((kv_other, 24, 128), BF16),
        vmem((16, 16, 128), BF16),
        vmem((256, 128), F32),
        vmem((2, 16, 128), BF16),
        vmem((tp_other, 16, 128), BF16),
    ]
    for n in (tp_other, kv_other, kv_other, kv_other, kv_other, kv_other, tp_other, kv_other, kv_other, tp_other):
        scratch += [dma((n,)), dma((n,))]
    return pl.pallas_call(
        functools.partial(kernel, n_kv, n_tp),
        out_shape=jax.ShapeDtypeStruct((16, 32), F32),
        in_specs=[pl.BlockSpec(memory_space=pl.ANY)] * len(args),
        out_specs=pl.BlockSpec(memory_space=pltpu.VMEM),
        scratch_shapes=scratch,
        compiler_params=pltpu.CompilerParams(
            collective_id=0, has_side_effects=True, vmem_limit_bytes=60 * 1024 * 1024
        ),
        name="layer_step",
    )(*args)


def solution(mesh):
    return jax.shard_map(
        functools.partial(on_device, mesh.shape["kv"], mesh.shape["tp"]),
        mesh=mesh,
        in_specs=(
            P(None, ("kv", "tp")),
            P("kv"),
            P("kv", "tp"),
            P("kv", "tp"),
            P("kv", "tp"),
            P("kv", None),
            P("tp"),
            P(None, "kv", "tp"),
            P(None, "kv", "tp"),
            P(None, "tp", "kv"),
            P("tp", "kv"),
            P("kv"),
            P("kv", "tp"),
            P("kv", "tp"),
            P("tp", "kv"),
        ),
        out_specs=P(None, ("kv", "tp")),
        check_vma=False,
    )
```

time: 145 us -> 58.2 us (0.40)
  blocking collectives: 85.3 us -> 0 us
  Pallas kernels: 0 us -> 55.3 us
  local copies, waits for them, and re-layouts: 23.3 us -> 2.71 us
  starting transfers between devices: 12.7 us -> 0 us
  matrix products: 11.2 us -> 0 us
  other arithmetic: 6.83 us -> 0 us
  waiting for transfers between devices: 4.64 us -> 0 us
    all_to_all x3 -> x0, blocking collectives: 65.8 us -> none  [sent_to_all(): lax.all_to_all(jnp.broadcast_to(value[None], (peers, *value.shape)), axis...]
    pallas_call x0 -> x1, Pallas kernels: none -> 55.3 us  [on_device(): pl.pallas_call(functools.partial(kernel, n_kv, n_tp), out_shape=jax.Shape...]
    all_gather x2 -> x0, blocking collectives: 19.4 us -> none  [collected_together(): both, at, found = (lax.all_gather(jnp.concatenate(lines), axis), 0, {})]
    all_to_all x2 -> x0, starting transfers between devices: 12.7 us -> none  [the longest x1 7.6 us: sent_to_all(): lax.all_to_all(jnp.broadcast_to(value[None], (peers, *value.shape)), axis...]
    unnamed x23 -> x2, local copies, waits for them, and re-layouts: 14 us -> 2.71 us
    dot_general x11 -> x0, matrix products: 11.2 us -> none  [the longest x1 3.47 us: on_device(): jnp.einsum('bgqp,bpgd->bgqd', weights.astype(jnp.bfloat16), value_rows, p...]
    reduce_sum x7 -> x0, other arithmetic: 4.82 us -> none  [the longest x2 4.04 us: over_copies(): return jnp.sum(everything, axis=0)]
    all_to_all x2 -> x0, waiting for transfers between devices: 4.64 us -> none  [the longest x1 4.64 us: sum_at_owner(): lax.all_to_all(parts, axis, split_axis=0, concat_axis=0, tiled=True)]
  transfers between devices with their start and end apart: 2 -> 0, of which waited for: 1 -> 0; matrix products, arithmetic and copies ran while one was open for 9% -> 0% of each run, Pallas kernels for 0% -> 0%
where the time goes in v1:
time: 58.2 us; the launch traced here: 58 us
  Pallas kernels  55.3 us (95%)
  local copies, waits for them, and re-layouts  2.71 us (5%)
    pallas_call x1, Pallas kernels, on_device(): pl.pallas_call(functools.partial(kernel, n_kv, n_tp), out_shape=jax.Shape...  55.3 us
    unnamed x2, local copies, waits for them, and re-layouts  2.71 us

profile of v1, /device:TPU:1, one launch (start us, length us, event | category | flops | bytes accessed | tf_op | source)
XLA Modules:
  0.0 58.0 jit_solution(12469993315949935547)
XLA Ops:
  0.0 1.4 %copy.16.w_forget = bf16[256,16]{1,0:T(8,128)(2,1)} copy(bf16[256,16]{0,1:T(8,128)(2,1)} %param.20) | data formatting | bytes 16384 | tf_op args[5]
  1.4 55.3 %layer_step.1 = f32[16,32]{1,0:T(8,128)} custom-call(bf16[16,32]{1,0:T(8,128)(2,1)} %hidden_in.1, f32[1,256]{1,0:T(1,128)} %bitcast.3, bf16[256,384]{1,0:T(8,128)(2,1)} %w_query.1, bf16[256,128]{1,0:T(8,128)(2,1)} %w_key.1, bf16[256,128]{1,0:T(8,128)(2,1)} %w_value.1, bf16[256,16]{1,0:T(8,128)(2,1)} %copy.16.w_forget, f32[1,2]{1,0:T(1,128)} %bitcast.5, ...), custom_call_target="tpu_custom_call" | custom-call | tf_op jit(solution)/shard_map/layer_step/pallas_call | solution.py:387
  56.7 1.3 %copy.18 = f32[16,32]{1,0:T(8,128)} copy(f32[16,32]{1,0:T(8,128)} %layer_step.1) | data formatting | bytes 4096

commit v2 on v1

--- a/solution.py
+++ b/solution.py
@@ -52,6 +52,7 @@
     wu,
     wd,
     load_sem,
+    plane,
     dec_rows,
     q_mine,
     q_in,
@@ -62,6 +63,9 @@
     q_rows,
     o_rows,
     l_rows,
+    own_rows,
+    top_rows,
+    sum_rows,
     a_mine,
     a_in,
     e_mine,
@@ -101,6 +105,15 @@
     kv_peers = [lax.rem(kv + d, n_kv) for d in range(1, n_kv)]
     tp_peers = [lax.rem(tp + d, n_tp) for d in range(1, n_tp)]
 
+    side = 4
+    z_line = [lax.rem(kv + side * d, n_kv) for d in range(1, n_kv // side)]
+    x_line = [kv // side * side + lax.rem(kv + d, side) for d in range(1, side)]
+    barrier = pltpu.get_barrier_semaphore()
+    for peer in tp_peers:
+        pl.semaphore_signal(barrier, inc=1, device_id={"kv": kv, "tp": peer}, device_id_type=MESH)
+    for peer in z_line + x_line:
+        pl.semaphore_signal(barrier, inc=1, device_id={"kv": peer, "tp": tp}, device_id_type=MESH)
+
     loads = [
         (hidden_in, xs.at[tp]),
         (pre_gain, pg),
@@ -123,43 +136,41 @@
         copy.start()
     (l_x, l_pg, l_wq, l_wk, l_wv, l_wf, l_fb, l_dec, l_kc, l_vc, l_wo, l_mg, l_wg, l_wu, l_wd) = loads
 
-    barrier = pltpu.get_barrier_semaphore()
-    for peer in kv_peers:
-        pl.semaphore_signal(barrier, inc=1, device_id={"kv": peer, "tp": tp}, device_id_type=MESH)
-    for peer in tp_peers:
-        pl.semaphore_signal(barrier, inc=1, device_id={"kv": kv, "tp": peer}, device_id_type=MESH)
-    pl.semaphore_wait(barrier, n_kv + n_tp - 2)
-
-    def send(axis, src, dst, send_sem, recv_sem):
+    def send(axis, src, dst, landed, send_sem, recv_sem):
         peers = kv_peers if axis == "kv" else tp_peers
-        copies = []
         for i, peer in enumerate(peers):
             device = {"kv": peer, "tp": tp} if axis == "kv" else {"kv": kv, "tp": peer}
-            copy = pltpu.make_async_remote_copy(
+            pltpu.make_async_remote_copy(
                 src_ref=src(peer),
                 dst_ref=dst(i),
-                send_sem=send_sem.at[i],
-                recv_sem=recv_sem.at[i],
+                send_sem=send_sem,
+                recv_sem=recv_sem,
                 device_id=device,
                 device_id_type=MESH,
-            )
-            copy.start()
-            copies.append(copy)
-        return copies
-
-    def received(copies):
-        for copy in copies:
-            copy.wait_recv()
-
-    def sent(copies):
-        for copy in copies:
-            copy.wait_send()
+            ).start()
+        return pltpu.make_async_remote_copy(
+            src_ref=landed,
+            dst_ref=landed,
+            send_sem=send_sem,
+            recv_sem=recv_sem,
+            device_id=device,
+            device_id_type=MESH,
+        )
+
+    def received(copy):
+        copy.wait_recv()
+
+    def sent(copy):
+        copy.wait_send()
 
     lane = lax.broadcasted_iota(jnp.int32, (16, 128), 1)
     low = lane < 64
 
+    pl.semaphore_wait(barrier, n_tp - 1 + len(z_line) + len(x_line))
+    for peer in x_line:
+        pl.semaphore_signal(plane, inc=1, device_id={"kv": peer, "tp": tp}, device_id_type=MESH)
     l_x.wait()
-    x_copies = send("tp", lambda peer: xs.at[tp], lambda i: xs.at[tp], x_send, x_recv)
+    x_copies = send("tp", lambda peer: xs.at[tp], lambda i: xs.at[tp], xs.at[pl.ds(0, n_tp - 1)], x_send, x_recv)
 
     q_rows[...] = jnp.zeros_like(q_rows)
     l_dec.wait()
@@ -177,12 +188,13 @@
     square = jnp.sum(x * x, axis=1, keepdims=True)
     square = jnp.broadcast_to(square, (16, 128))
     s_mine[...] = jnp.where(low[0:8], square[0:8], square[8:16])
-    q_copies = send("kv", lambda peer: q_mine, lambda i: q_in.at[i], q_send, q_recv)
-    s_copies = send("kv", lambda peer: s_mine, lambda i: s_in.at[i], s_send, s_recv)
+    pl.semaphore_wait(plane, len(x_line))
+    q_copies = send("kv", lambda peer: q_mine, lambda i: q_in.at[i], q_in, q_send, q_recv)
+    s_copies = send("kv", lambda peer: s_mine, lambda i: s_in.at[i], s_in, s_send, s_recv)
 
     k_part = jnp.dot(scaled, wk[...], preferred_element_type=F32)
     v_part = jnp.dot(scaled, wv[...], preferred_element_type=F32)
-    f_part = jnp.dot(scaled, wf[...], preferred_element_type=F32)
+    f_part = lax.dot_general(scaled, wf[...], (((1,), (1,)), ((), ())), preferred_element_type=F32)
     f_col = lax.broadcasted_iota(jnp.int32, (16, 16), 1)
     f_zero = jnp.zeros_like(f_part)
     f_first = jnp.sum(jnp.where(f_col == 2 * tp, f_part, f_zero), axis=1, keepdims=True)
@@ -193,7 +205,7 @@
     t_mine[pl.ds(2, 16, stride=8), :] = f_wide
     t_mine[pl.ds(3, 16, stride=8), :] = square
     t_copies = send(
-        "kv", lambda peer: t_mine.at[pl.ds(pl.multiple_of(peer * 8, 8), 8)], lambda i: t_in.at[i], t_send, t_recv
+        "kv", lambda peer: t_mine.at[pl.ds(pl.multiple_of(peer * 8, 8), 8)], lambda i: t_in.at[i], t_in, t_send, t_recv
     )
     sent(x_copies)
     l_kc.wait()
@@ -232,19 +244,32 @@
     own = jnp.sum(q_own * key_new, axis=1, keepdims=True)
     own = own - jnp.where(row8[:, 0:1] < 3, log_new[:, 0:1], log_new[:, 64:65])
 
-    for b in range(16):
-        q8 = q_rows[b * 8 : (b + 1) * 8, :].astype(BF16)
+    own_here = jnp.broadcast_to(own, (8, 128))
+    absent = jnp.full((8, 128), -jnp.inf, F32)
+    for b in range(16):
+        own_rows[8 * b : 8 * (b + 1), :] = jnp.where(kv == b, own_here, absent)
+    for b in range(16):
+        q8 = q_rows[8 * b : 8 * (b + 1), :].astype(BF16)
         scores = lax.dot_general(q8, kc[b], (((1,), (1,)), ((), ())), preferred_element_type=F32)
         scores = scores + dec_rows[b]
-        own_b = jnp.where(kv == b, own, -jnp.inf)
-        top = jnp.maximum(jnp.max(scores, axis=1, keepdims=True), own_b)
-        weights = jnp.exp(scores - top)
-        own_weight = jnp.exp(own_b - top)
-        total = jnp.sum(weights, axis=1, keepdims=True) + own_weight
-        mixed = jnp.dot(weights.astype(BF16), vc[b], preferred_element_type=F32)
-        mixed = mixed + own_weight * value_new
-        o_rows[b * 8 : (b + 1) * 8, :] = mixed / total
-        l_rows[b * 8 : (b + 1) * 8, :] = jnp.broadcast_to(top + jnp.log(total), (8, 128))
+        top_rows[8 * b : 8 * (b + 1), :] = functools.reduce(
+            jnp.maximum, [scores[:, 128 * j : 128 * (j + 1)] for j in range(8)]
+        )
+        dec_rows[b] = scores
+    own_all = own_rows[...]
+    top = jnp.maximum(jnp.max(top_rows[...], axis=1, keepdims=True), own_all)
+    top_rows[...] = top
+    for b in range(16):
+        top_b = top_rows[8 * b : 8 * (b + 1), :]
+        weights = jnp.exp(dec_rows[b] - jnp.concatenate([top_b] * 8, axis=1))
+        sum_rows[8 * b : 8 * (b + 1), :] = functools.reduce(
+            jnp.add, [weights[:, 128 * j : 128 * (j + 1)] for j in range(8)]
+        )
+        o_rows[8 * b : 8 * (b + 1), :] = jnp.dot(weights.astype(BF16), vc[b], preferred_element_type=F32)
+    own_weight = jnp.exp(own_all - top)
+    total = jnp.sum(sum_rows[...], axis=1, keepdims=True) + own_weight
+    o_rows[...] = (o_rows[...] + own_weight * value_new) / total
+    l_rows[...] = top + jnp.log(total)
 
     heads = [o_rows[pl.ds(h, 16, stride=8), :] for h in range(6)]
     logs = [l_rows[pl.ds(h, 16, stride=8), :] for h in range(6)]
@@ -253,12 +278,14 @@
     chunk_2 = jnp.where(low, pltpu.roll(heads[4], 64, 1), heads[5])
     mine = jnp.concatenate([chunk_0, chunk_1, chunk_2], axis=1).astype(BF16)
     a_mine[...] = mine
+    spot = lax.rem(lane, 64)
     e_wide = logs[0]
     for h in range(1, 6):
-        e_wide = jnp.where(lane < 16 * h, e_wide, logs[h])
+        e_wide = jnp.where(spot < 8 * h, e_wide, logs[h])
+    e_wide = jnp.where(low[0:8], e_wide[0:8], e_wide[8:16])
     e_mine[...] = e_wide
-    e_copies = send("kv", lambda peer: e_mine, lambda i: e_in.at[i], e_send, e_recv)
-    a_copies = send("kv", lambda peer: a_mine, lambda i: a_in.at[i], a_send, a_recv)
+    e_copies = send("kv", lambda peer: e_mine, lambda i: e_in.at[i], e_in, e_send, e_recv)
+    a_copies = send("kv", lambda peer: a_mine, lambda i: a_in.at[i], a_in, a_send, a_recv)
     sent(q_copies)
     sent(s_copies)
     sent(t_copies)
@@ -273,22 +300,17 @@
     attended = jnp.zeros((16, 384), F32)
     for i in range(n_kv):
         share = shares[i] * inverse
-        wide = jnp.concatenate(
-            [jnp.broadcast_to(share[:, 16 * h : 16 * h + 1], (16, 128)) for h in range(6)], axis=1
-        )
-        wide = jnp.concatenate(
-            [
-                jnp.where(low, wide[:, 256 * c : 256 * c + 128], wide[:, 256 * c + 128 : 256 * c + 256])
-                for c in range(3)
-            ],
-            axis=1,
-        )
+        wide = [
+            jnp.concatenate([jnp.broadcast_to(share[:, at : at + 1], (8, 128)) for at in (8 * h, 64 + 8 * h)], axis=0)
+            for h in range(6)
+        ]
+        wide = jnp.concatenate([jnp.where(low, wide[2 * c], wide[2 * c + 1]) for c in range(3)], axis=1)
         value = mine if i == 0 else a_in[i - 1]
         attended = attended + wide * value.astype(F32)
 
     part = jnp.dot(attended.astype(BF16), wo[...], preferred_element_type=F32).astype(BF16)
     p_mine[...] = part
-    p_copies = send("tp", lambda peer: p_mine, lambda i: p_in.at[i], p_send, p_recv)
+    p_copies = send("tp", lambda peer: p_mine, lambda i: p_in.at[i], p_in, p_send, p_recv)
     sent(e_copies)
     sent(a_copies)
     for copy in (l_mg, l_wg, l_wu, l_wd):
@@ -310,7 +332,7 @@
     g_rows[pl.ds(23, 16, stride=24), :] = mid_square - square_high
     for b in range(16):
         g_mine[b] = g_rows[24 * b : 24 * (b + 1), :].astype(BF16)
-    g_copies = send("kv", lambda peer: g_mine.at[peer], lambda i: g_in.at[i], g_send, g_recv)
+    g_copies = send("kv", lambda peer: g_mine.at[peer], lambda i: g_in.at[i], g_in, g_send, g_recv)
     sent(p_copies)
     received(g_copies)
     g_sum = g_mine[kv].astype(F32)
@@ -322,7 +344,7 @@
     hidden = gate / (1.0 + jnp.exp(-gate)) * up
     hidden = jnp.concatenate([hidden, jnp.zeros((5, 128), F32)], axis=0).astype(BF16)
     h_all[kv] = hidden
-    h_copies = send("kv", lambda peer: h_all.at[kv], lambda i: h_all.at[kv], h_send, h_recv)
+    h_copies = send("kv", lambda peer: h_all.at[kv], lambda i: h_all.at[kv], h_all.at[pl.ds(0, n_kv - 1)], h_send, h_recv)
     sent(g_copies)
     received(h_copies)
     for b in range(16):
@@ -331,7 +353,7 @@
     down = jnp.dot(units, wd[...], preferred_element_type=F32).astype(BF16)
     d_mine[0] = down[:, 0:128]
     d_mine[1] = down[:, 128:256]
-    d_copies = send("tp", lambda peer: d_mine.at[peer // 4], lambda i: d_in.at[i], d_send, d_recv)
+    d_copies = send("tp", lambda peer: d_mine.at[peer // 4], lambda i: d_in.at[i], d_in, d_send, d_recv)
     sent(h_copies)
     result = d_mine[tp // 4].astype(F32)
     received(d_copies)
@@ -350,6 +372,7 @@
     args = list(args)
     for i in (1, 6, 11):
         args[i] = args[i].reshape(1, -1)
+    args[5] = args[5].T
     vmem = pltpu.VMEM
     own = [vmem(a.shape, a.dtype) for a in args[1:]]
     kv_other, tp_other = n_kv - 1, n_tp - 1
@@ -358,6 +381,7 @@
         vmem((n_tp, 16, 32), BF16),
         *own,
         dma((15,)),
+        pltpu.SemaphoreType.REGULAR,
         vmem((16, 8, 1024), F32),
         vmem((16, 384), F32),
         vmem((kv_other, 16, 384), F32),
@@ -368,10 +392,13 @@
         vmem((128, 128), F32),
         vmem((128, 128), F32),
         vmem((128, 128), F32),
+        vmem((128, 128), F32),
+        vmem((128, 128), F32),
+        vmem((128, 128), F32),
         vmem((16, 384), BF16),
         vmem((kv_other, 16, 384), BF16),
-        vmem((16, 128), F32),
-        vmem((kv_other, 16, 128), F32),
+        vmem((8, 128), F32),
+        vmem((kv_other, 8, 128), F32),
         vmem((16, 256), BF16),
         vmem((tp_other, 16, 256), BF16),
         vmem((16 * 24, 128), F32),
@@ -382,13 +409,11 @@
         vmem((2, 16, 128), BF16),
         vmem((tp_other, 16, 128), BF16),
     ]
-    for n in (tp_other, kv_other, kv_other, kv_other, kv_other, kv_other, tp_other, kv_other, kv_other, tp_other):
-        scratch += [dma((n,)), dma((n,))]
+    scratch += [dma] * 20
     return pl.pallas_call(
         functools.partial(kernel, n_kv, n_tp),
-        out_shape=jax.ShapeDtypeStruct((16, 32), F32),
+        out_shape=vmem((16, 32), F32),
         in_specs=[pl.BlockSpec(memory_space=pl.ANY)] * len(args),
-        out_specs=pl.BlockSpec(memory_space=pltpu.VMEM),
         scratch_shapes=scratch,
         compiler_params=pltpu.CompilerParams(
             collective_id=0, has_side_effects=True, vmem_limit_bytes=60 * 1024 * 1024

time: 58.2 us -> 47.2 us (0.81)
  Pallas kernels: 55.3 us -> 46.5 us
  local copies, waits for them, and re-layouts: 2.71 us -> 0.6 us
    pallas_call x1, Pallas kernels: 55.3 us -> 46.5 us  [on_device(): pl.pallas_call(functools.partial(kernel, n_kv, n_tp), out_shape=vmem((16,...]
    unnamed x2 -> x1, local copies, waits for them, and re-layouts: 2.71 us -> 0.6 us
where the time goes in v2:
time: 47.2 us; the launch traced here: 47.1 us
  Pallas kernels  46.5 us (99%)
  local copies, waits for them, and re-layouts  0.6 us (1%)
    pallas_call x1, Pallas kernels, on_device(): pl.pallas_call(functools.partial(kernel, n_kv, n_tp), out_shape=vmem((16,...  46.5 us

profile of v2, /device:TPU:1, one launch (start us, length us, event | category | flops | bytes accessed | tf_op | source)
XLA Modules:
  0.0 47.1 jit_solution(15945500363229597999)
XLA Ops:
  0.0 46.5 %layer_step.1 = f32[16,32]{1,0:T(8,128)S(1)} custom-call(bf16[16,32]{1,0:T(8,128)(2,1)} %hidden_in.1, f32[1,256]{1,0:T(1,128)} %bitcast.5, bf16[256,384]{1,0:T(8,128)(2,1)} %w_query.1, bf16[256,128]{1,0:T(8,128)(2,1)} %w_key.1, bf16[256,128]{1,0:T(8,128)(2,1)} %w_value.1, bf16[16,256]{1,0:T(8,128)(2,1)} %bitcast.4, f32[1,2]{1,0:T(1,128)} %bitcast.7, ...), custom_call_target="tpu_custom_call" | custom-call | tf_op jit(solution)/shard_map/layer_step/pallas_call | solution.py:413
  46.5 0.6 %copy.17 = f32[16,32]{1,0:T(8,128)} copy(f32[16,32]{1,0:T(8,128)S(1)} %layer_step.1) | data formatting | bytes 4096

commit v3 on v2

--- a/solution.py
+++ b/solution.py
@@ -56,8 +56,12 @@
     dec_rows,
     q_mine,
     q_in,
+    q_line,
+    u_in,
     s_mine,
     s_in,
+    s_line,
+    w_in,
     t_mine,
     t_in,
     q_rows,
@@ -83,6 +87,10 @@
     x_recv,
     q_send,
     q_recv,
+    u_send,
+    u_recv,
+    w_send,
+    w_recv,
     s_send,
     s_recv,
     t_send,
@@ -102,12 +110,21 @@
 ):
     kv = lax.axis_index("kv")
     tp = lax.axis_index("tp")
-    kv_peers = [lax.rem(kv + d, n_kv) for d in range(1, n_kv)]
-    tp_peers = [lax.rem(tp + d, n_tp) for d in range(1, n_tp)]
-
     side = 4
-    z_line = [lax.rem(kv + side * d, n_kv) for d in range(1, n_kv // side)]
-    x_line = [kv // side * side + lax.rem(kv + d, side) for d in range(1, side)]
+    z, x_at, y, core = kv // side, lax.rem(kv, side), tp // 2, lax.rem(tp, 2)
+
+    def far(d):
+        return min(d, side - d)
+
+    steps = [(dz, dx) for dz in range(side) for dx in range(side) if dz or dx]
+    steps.sort(key=lambda s: -far(s[0]) - far(s[1]))
+    kv_peers = [lax.rem(z + dz, side) * side + lax.rem(x_at + dx, side) for dz, dx in steps]
+    steps = [(dy, dc) for dy in range(n_tp // 2) for dc in range(2) if dy or dc]
+    steps.sort(key=lambda s: -2 * far(s[0]) - s[1])
+    tp_peers = [lax.rem(y + dy, n_tp // 2) * 2 + lax.rem(core + dc, 2) for dy, dc in steps]
+
+    z_line = [lax.rem(z + d, side) * side + x_at for d in (2, 1, 3)]
+    x_line = [z * side + lax.rem(x_at + d, side) for d in (2, 1, 3)]
     barrier = pltpu.get_barrier_semaphore()
     for peer in tp_peers:
         pl.semaphore_signal(barrier, inc=1, device_id={"kv": kv, "tp": peer}, device_id_type=MESH)
@@ -137,9 +154,9 @@
     (l_x, l_pg, l_wq, l_wk, l_wv, l_wf, l_fb, l_dec, l_kc, l_vc, l_wo, l_mg, l_wg, l_wu, l_wd) = loads
 
     def send(axis, src, dst, landed, send_sem, recv_sem):
-        peers = kv_peers if axis == "kv" else tp_peers
+        peers = {"kv": kv_peers, "tp": tp_peers, "z": z_line, "x": x_line}[axis]
         for i, peer in enumerate(peers):
-            device = {"kv": peer, "tp": tp} if axis == "kv" else {"kv": kv, "tp": peer}
+            device = {"kv": kv, "tp": peer} if axis == "tp" else {"kv": peer, "tp": tp}
             pltpu.make_async_remote_copy(
                 src_ref=src(peer),
                 dst_ref=dst(i),
@@ -188,9 +205,8 @@
     square = jnp.sum(x * x, axis=1, keepdims=True)
     square = jnp.broadcast_to(square, (16, 128))
     s_mine[...] = jnp.where(low[0:8], square[0:8], square[8:16])
-    pl.semaphore_wait(plane, len(x_line))
-    q_copies = send("kv", lambda peer: q_mine, lambda i: q_in.at[i], q_in, q_send, q_recv)
-    s_copies = send("kv", lambda peer: s_mine, lambda i: s_in.at[i], s_in, s_send, s_recv)
+    q_copies = send("z", lambda peer: q_mine, lambda i: q_in.at[i], q_in, q_send, q_recv)
+    s_copies = send("z", lambda peer: s_mine, lambda i: s_in.at[i], s_in, s_send, s_recv)
 
     k_part = jnp.dot(scaled, wk[...], preferred_element_type=F32)
     v_part = jnp.dot(scaled, wv[...], preferred_element_type=F32)
@@ -204,20 +220,32 @@
     t_mine[pl.ds(1, 16, stride=8), :] = v_part
     t_mine[pl.ds(2, 16, stride=8), :] = f_wide
     t_mine[pl.ds(3, 16, stride=8), :] = square
-    t_copies = send(
-        "kv", lambda peer: t_mine.at[pl.ds(pl.multiple_of(peer * 8, 8), 8)], lambda i: t_in.at[i], t_in, t_send, t_recv
-    )
     sent(x_copies)
-    l_kc.wait()
-    l_vc.wait()
-
     received(q_copies)
     received(s_copies)
     q_sum = q_mine[...]
     s_sum = s_mine[...]
-    for i in range(n_kv - 1):
+    for i in range(side - 1):
         q_sum = q_sum + q_in[i]
         s_sum = s_sum + s_in[i]
+    q_line[...] = q_sum
+    s_line[...] = s_sum
+    u_copies = send("x", lambda peer: q_line, lambda i: u_in.at[i], u_in, u_send, u_recv)
+    w_copies = send("x", lambda peer: s_line, lambda i: w_in.at[i], w_in, w_send, w_recv)
+    pl.semaphore_wait(plane, len(x_line))
+    t_copies = send(
+        "kv", lambda peer: t_mine.at[pl.ds(pl.multiple_of(peer * 8, 8), 8)], lambda i: t_in.at[i], t_in, t_send, t_recv
+    )
+    l_kc.wait()
+    l_vc.wait()
+    sent(q_copies)
+    sent(s_copies)
+
+    received(u_copies)
+    received(w_copies)
+    for i in range(side - 1):
+        q_sum = q_sum + u_in[i]
+        s_sum = s_sum + w_in[i]
     s_sum = jnp.concatenate([s_sum[:, 0:1], s_sum[:, 64:65]], axis=0)
     inv_rms = lax.rsqrt(s_sum / D + NORM_EPS)
     query = (q_sum * inv_rms).astype(BF16).astype(F32) * (HD**-0.5)
@@ -228,6 +256,15 @@
         if half != g:
             part = pltpu.roll(part, 64, 1)
         q_rows[pl.ds(h, 16, stride=8), :] = jnp.where(low if g == 0 else ~low, part, zero)
+
+    for b in range(16):
+        q8 = q_rows[8 * b : 8 * (b + 1), :].astype(BF16)
+        scores = lax.dot_general(q8, kc[b], (((1,), (1,)), ((), ())), preferred_element_type=F32)
+        scores = scores + dec_rows[b]
+        top_rows[8 * b : 8 * (b + 1), :] = functools.reduce(
+            jnp.maximum, [scores[:, 128 * j : 128 * (j + 1)] for j in range(8)]
+        )
+        dec_rows[b] = scores
 
     received(t_copies)
     t_sum = t_mine[pl.ds(pl.multiple_of(kv * 8, 8), 8), :]
@@ -248,14 +285,6 @@
     absent = jnp.full((8, 128), -jnp.inf, F32)
     for b in range(16):
         own_rows[8 * b : 8 * (b + 1), :] = jnp.where(kv == b, own_here, absent)
-    for b in range(16):
-        q8 = q_rows[8 * b : 8 * (b + 1), :].astype(BF16)
-        scores = lax.dot_general(q8, kc[b], (((1,), (1,)), ((), ())), preferred_element_type=F32)
-        scores = scores + dec_rows[b]
-        top_rows[8 * b : 8 * (b + 1), :] = functools.reduce(
-            jnp.maximum, [scores[:, 128 * j : 128 * (j + 1)] for j in range(8)]
-        )
-        dec_rows[b] = scores
     own_all = own_rows[...]
     top = jnp.maximum(jnp.max(top_rows[...], axis=1, keepdims=True), own_all)
     top_rows[...] = top
@@ -286,8 +315,8 @@
     e_mine[...] = e_wide
     e_copies = send("kv", lambda peer: e_mine, lambda i: e_in.at[i], e_in, e_send, e_recv)
     a_copies = send("kv", lambda peer: a_mine, lambda i: a_in.at[i], a_in, a_send, a_recv)
-    sent(q_copies)
-    sent(s_copies)
+    sent(u_copies)
+    sent(w_copies)
     sent(t_copies)
     received(e_copies)
     parts = [e_wide] + [e_in[i] for i in range(n_kv - 1)]
@@ -384,9 +413,13 @@
         pltpu.SemaphoreType.REGULAR,
         vmem((16, 8, 1024), F32),
         vmem((16, 384), F32),
-        vmem((kv_other, 16, 384), F32),
+        vmem((3, 16, 384), F32),
+        vmem((16, 384), F32),
+        vmem((3, 16, 384), F32),
         vmem((8, 128), F32),
-        vmem((kv_other, 8, 128), F32),
+        vmem((3, 8, 128), F32),
+        vmem((8, 128), F32),
+        vmem((3, 8, 128), F32),
         vmem((128, 128), F32),
         vmem((kv_other, 8, 128), F32),
         vmem((128, 128), F32),
@@ -409,7 +442,7 @@
         vmem((2, 16, 128), BF16),
         vmem((tp_other, 16, 128), BF16),
     ]
-    scratch += [dma] * 20
+    scratch += [dma] * 24
     return pl.pallas_call(
         functools.partial(kernel, n_kv, n_tp),
         out_shape=vmem((16, 32), F32),

time: 47.2 us -> 45.2 us (0.958)
  Pallas kernels: 46.5 us -> 44.5 us
    pallas_call x1, Pallas kernels: 46.5 us -> 44.5 us  [on_device(): pl.pallas_call(functools.partial(kernel, n_kv, n_tp), out_shape=vmem((16,...]
where the time goes in v3:
time: 45.2 us; the launch traced here: 45.1 us
  Pallas kernels  44.5 us (98%)
  local copies, waits for them, and re-layouts  0.6 us (1%)
    pallas_call x1, Pallas kernels, on_device(): pl.pallas_call(functools.partial(kernel, n_kv, n_tp), out_shape=vmem((16,...  44.5 us

profile of v3, /device:TPU:1, one launch (start us, length us, event | category | flops | bytes accessed | tf_op | source)
XLA Modules:
  0.0 45.1 jit_solution(8817483272422100802)
XLA Ops:
  0.0 44.5 %layer_step.1 = f32[16,32]{1,0:T(8,128)S(1)} custom-call(bf16[16,32]{1,0:T(8,128)(2,1)} %hidden_in.1, f32[1,256]{1,0:T(1,128)} %bitcast.5, bf16[256,384]{1,0:T(8,128)(2,1)} %w_query.1, bf16[256,128]{1,0:T(8,128)(2,1)} %w_key.1, bf16[256,128]{1,0:T(8,128)(2,1)} %w_value.1, bf16[16,256]{1,0:T(8,128)(2,1)} %bitcast.4, f32[1,2]{1,0:T(1,128)} %bitcast.7, ...), custom_call_target="tpu_custom_call" | custom-call | tf_op jit(solution)/shard_map/layer_step/pallas_call | solution.py:446
  44.5 0.6 %copy.17 = f32[16,32]{1,0:T(8,128)} copy(f32[16,32]{1,0:T(8,128)S(1)} %layer_step.1) | data formatting | bytes 4096

commit v4 on v3

--- a/solution.py
+++ b/solution.py
@@ -70,6 +70,7 @@
     own_rows,
     top_rows,
     sum_rows,
+    w_rows,
     a_mine,
     a_in,
     e_mine,
@@ -294,19 +295,11 @@
         sum_rows[8 * b : 8 * (b + 1), :] = functools.reduce(
             jnp.add, [weights[:, 128 * j : 128 * (j + 1)] for j in range(8)]
         )
-        o_rows[8 * b : 8 * (b + 1), :] = jnp.dot(weights.astype(BF16), vc[b], preferred_element_type=F32)
+        w_rows[b] = weights.astype(BF16)
     own_weight = jnp.exp(own_all - top)
     total = jnp.sum(sum_rows[...], axis=1, keepdims=True) + own_weight
-    o_rows[...] = (o_rows[...] + own_weight * value_new) / total
     l_rows[...] = top + jnp.log(total)
-
-    heads = [o_rows[pl.ds(h, 16, stride=8), :] for h in range(6)]
     logs = [l_rows[pl.ds(h, 16, stride=8), :] for h in range(6)]
-    chunk_0 = jnp.where(low, heads[0], pltpu.roll(heads[1], 64, 1))
-    chunk_1 = jnp.where(low, heads[2], heads[3])
-    chunk_2 = jnp.where(low, pltpu.roll(heads[4], 64, 1), heads[5])
-    mine = jnp.concatenate([chunk_0, chunk_1, chunk_2], axis=1).astype(BF16)
-    a_mine[...] = mine
     spot = lax.rem(lane, 64)
     e_wide = logs[0]
     for h in range(1, 6):
@@ -314,6 +307,16 @@
     e_wide = jnp.where(low[0:8], e_wide[0:8], e_wide[8:16])
     e_mine[...] = e_wide
     e_copies = send("kv", lambda peer: e_mine, lambda i: e_in.at[i], e_in, e_send, e_recv)
+    for b in range(16):
+        o_rows[8 * b : 8 * (b + 1), :] = jnp.dot(w_rows[b], vc[b], preferred_element_type=F32)
+    o_rows[...] = (o_rows[...] + own_weight * value_new) / total
+
+    heads = [o_rows[pl.ds(h, 16, stride=8), :] for h in range(6)]
+    chunk_0 = jnp.where(low, heads[0], pltpu.roll(heads[1], 64, 1))
+    chunk_1 = jnp.where(low, heads[2], heads[3])
+    chunk_2 = jnp.where(low, pltpu.roll(heads[4], 64, 1), heads[5])
+    mine = jnp.concatenate([chunk_0, chunk_1, chunk_2], axis=1).astype(BF16)
+    a_mine[...] = mine
     a_copies = send("kv", lambda peer: a_mine, lambda i: a_in.at[i], a_in, a_send, a_recv)
     sent(u_copies)
     sent(w_copies)
@@ -428,6 +431,7 @@
         vmem((128, 128), F32),
         vmem((128, 128), F32),
         vmem((128, 128), F32),
+        vmem((16, 8, 1024), BF16),
         vmem((16, 384), BF16),
         vmem((kv_other, 16, 384), BF16),
         vmem((8, 128), F32),

time: 45.2 us -> 45.1 us (level)
  no operation moved by 1% of the time
where the time goes in v4:
time: 45.1 us; the launch traced here: 45 us
  Pallas kernels  44.4 us (98%)
  local copies, waits for them, and re-layouts  0.6 us (1%)
    pallas_call x1, Pallas kernels, on_device(): pl.pallas_call(functools.partial(kernel, n_kv, n_tp), out_shape=vmem((16,...  44.4 us

profile of v4, /device:TPU:1, one launch (start us, length us, event | category | flops | bytes accessed | tf_op | source)
XLA Modules:
  0.0 45.0 jit_solution(16945258296260246208)
XLA Ops:
  0.0 44.4 %layer_step.1 = f32[16,32]{1,0:T(8,128)S(1)} custom-call(bf16[16,32]{1,0:T(8,128)(2,1)} %hidden_in.1, f32[1,256]{1,0:T(1,128)} %bitcast.5, bf16[256,384]{1,0:T(8,128)(2,1)} %w_query.1, bf16[256,128]{1,0:T(8,128)(2,1)} %w_key.1, bf16[256,128]{1,0:T(8,128)(2,1)} %w_value.1, bf16[16,256]{1,0:T(8,128)(2,1)} %bitcast.4, f32[1,2]{1,0:T(1,128)} %bitcast.7, ...), custom_call_target="tpu_custom_call" | custom-call | tf_op jit(solution)/shard_map/layer_step/pallas_call | solution.py:450
  44.4 0.6 %copy.17 = f32[16,32]{1,0:T(8,128)} copy(f32[16,32]{1,0:T(8,128)S(1)} %layer_step.1) | data formatting | bytes 4096
